TPU v7x, 512 devices: a 4x2x32 block of a 4x8x32 slice. The times are simulated.
512 devices in a mesh: grp: 2 (over y), sp: 32 (over z), tp: 8 (over x, core).
Axes of the slice: x: 4, y: 2, z: 32, core: 2. Of those that a mesh axis runs over, the one named last changes fastest.
The devices are a block of a 4x8x32 slice.
Arguments:
- tokens: bfloat16 [16384, 4096], P(('grp', 'sp', 'tp')), parts along dimension 0, may hold values from -8 to 8
- input_gain: float32 [4096], replicated, may hold values from 0.1 to 1.9
- w_query: bfloat16 [4096, 2048], P('sp', 'tp'), may hold values from -0.09375 to 0.09375
- w_key: bfloat16 [4096, 512], P('sp'), may hold values from -0.09375 to 0.09375
- w_value: bfloat16 [4096, 512], P('sp'), may hold values from -0.09375 to 0.09375
- query_gain: float32 [128], replicated, may hold values from 0.1 to 17
- key_gain: float32 [128], replicated, may hold values from 0.1 to 15
- w_out: bfloat16 [2048, 4096], P('tp', 'sp'), may hold values from -0.5 to 0.5
Outputs:
- mixed: bfloat16 [16384, 4096], P(('grp', 'sp', 'tp')), parts along dimension 0
There are 2 independent parts, one for each index of `grp`. A program takes and returns all parts, laid end to end along the dimension named above; an argument that names none is the same for every part. Nothing has to cross between parts.
All inputs are finite; a program needn't handle non-finite values.
Results may differ from a plain program's by a relative error of at most 0.02.
The roundings to bfloat16 on the way count: a program that leaves them out, or rounds other values in their place, can miss the bound.
Values may be sent and summed in bfloat16 or wider, within the bound.
A program may use at most 64 MiB of HBM per device.

v0:
```python
import jax
import jax.numpy as jnp
from jax import lax
from jax.sharding import PartitionSpec as P

HEAD = 128
GRID_W = 64


eps = 1e-06


def sent_together(arrays, axis, dim, along):
    ends, at = ([], 0)
    for a in arrays[:-1]:
        at += a.shape[along]
        ends.append(at)
    both = jnp.concatenate(arrays, axis=along)
    return tuple(jnp.split(lax.all_gather(both, axis, axis=dim, tiled=True), ends, axis=along))


def sent_to_all(value, axis):
    copies = jnp.broadcast_to(value, (lax.axis_size(axis), *value.shape))
    return lax.all_to_all(copies, axis, split_axis=0, concat_axis=0, tiled=True)


def joined_along(pieces, dim):
    dims = list(pieces.shape[1:])
    dims[dim] *= pieces.shape[0]
    return jnp.moveaxis(pieces, 0, dim).reshape(dims)


def collect(value, axis, dim):
    pieces = sent_to_all(value, axis)
    return joined_along(pieces, dim)


def cut_along(value, dim, length):
    before, after = (value.shape[:dim], value.shape[dim + 1 :])
    return jnp.moveaxis(value.reshape(*before, length, -1, *after), dim, 0)


def sent_and_summed(value, axis, dim):
    pieces = cut_along(value, dim, lax.axis_size(axis))
    arrived = lax.all_to_all(pieces, axis, split_axis=0, concat_axis=0, tiled=True)
    return arrived.astype(jnp.float32).sum(axis=0)


def rms_rows(values, gain):
    floats = values.astype(jnp.float32)
    scale = lax.rsqrt(jnp.mean(floats * floats, axis=-1, keepdims=True) + eps)
    return floats * scale * gain


def rotate_half(part, angles):
    first, second = jnp.split(part, 2, axis=-1)
    cosine = jnp.cos(angles)
    sine = jnp.sin(angles)
    return jnp.concatenate(
        [first * cosine - second * sine, second * cosine + first * sine], axis=-1
    )


def turn_heads(heads, gain, positions):
    normed = rms_rows(heads, gain)
    quarter = heads.shape[-1] // 4
    inverse = 10000.0 ** (-jnp.arange(quarter, dtype=jnp.float32) * 2.0 / (2 * quarter))
    grid_row = (positions // GRID_W).astype(jnp.float32)
    grid_col = (positions % GRID_W).astype(jnp.float32)
    row_angle = (grid_row[:, None] * inverse[None, :])[:, None, :]
    col_angle = (grid_col[:, None] * inverse[None, :])[:, None, :]
    row_part, col_part = jnp.split(normed, 2, axis=-1)
    return jnp.concatenate(
        [rotate_half(row_part, row_angle), rotate_half(col_part, col_angle)], axis=-1
    )


def turn_keys(raw_keys, key_gain, positions):
    return turn_heads(raw_keys[:, None, :], key_gain, positions)[:, 0, :].astype(jnp.bfloat16)


def local(tokens, input_gain, w_query, w_key, w_value, query_gain, key_gain, w_out):
    local_rows = tokens.shape[0]
    tp_count = lax.axis_size("tp")
    rows = local_rows * tp_count
    first_row = lax.axis_index("sp") * rows
    tp_rank = lax.axis_index("tp")
    full_query, full_key, full_value = sent_together((w_query, w_key, w_value), "sp", 0, 1)
    kv_count = full_key.shape[1] // HEAD
    kv_index = tp_rank // (tp_count // kv_count)
    head_key = lax.dynamic_slice_in_dim(full_key, kv_index * HEAD, HEAD, 1)
    head_value = lax.dynamic_slice_in_dim(full_value, kv_index * HEAD, HEAD, 1)
    query_cols = full_query.shape[1]
    normed = rms_rows(collect(tokens, "tp", 0), input_gain).astype(jnp.bfloat16)
    projected = jnp.concatenate(
        [
            jnp.dot(normed, full_query, preferred_element_type=jnp.float32),
            jnp.dot(normed, head_key, preferred_element_type=jnp.float32),
            jnp.dot(normed, head_value, preferred_element_type=jnp.float32),
        ],
        axis=1,
    ).astype(jnp.bfloat16)
    query = projected[:, :query_cols]
    key_head = projected[:, query_cols : query_cols + HEAD]
    value_head = projected[:, query_cols + HEAD :]
    local_heads = query_cols // HEAD
    positions = first_row + jnp.arange(rows, dtype=jnp.int32)
    turned_query = (
        turn_heads(query.reshape(rows, local_heads, HEAD), query_gain, positions) * HEAD ** (-0.5)
    ).astype(jnp.bfloat16)
    query_rows = turned_query.transpose(1, 0, 2).reshape(local_heads * rows, HEAD)
    query_count = local_heads * rows
    piece = sent_together((key_head, value_head), "sp", 0, 1)
    where = jnp.arange(piece[0].shape[0], dtype=jnp.int32)
    peak = jnp.full((query_count,), -1e30, jnp.float32)
    scores = lax.dot_general(
        query_rows,
        turn_keys(piece[0], key_gain, where),
        (((1,), (1,)), ((), ())),
        preferred_element_type=jnp.float32,
    )
    new_peak = jnp.maximum(peak, jnp.max(scores, axis=1))
    weights = jnp.exp(scores - new_peak[:, None])
    total = jnp.sum(weights, axis=1)
    summed = jnp.dot(weights.astype(jnp.bfloat16), piece[1], preferred_element_type=jnp.float32)
    peak, total, summed = (new_peak, total, summed)
    attended = (summed / total[:, None]).astype(jnp.bfloat16)
    attended = (
        attended.reshape(local_heads, rows, HEAD).transpose(1, 0, 2).reshape(rows, query_cols)
    )
    full_out = lax.all_gather(w_out, "sp", axis=1, tiled=True)
    partial_value = jnp.dot(attended, full_out, preferred_element_type=jnp.float32)
    return sent_and_summed(
        lax.optimization_barrier(partial_value.astype(jnp.bfloat16))
        .astype(jnp.float32)
        .astype(jnp.bfloat16),
        "tp",
        0,
    ).astype(jnp.bfloat16)


def solution(mesh):
    in_specs = (
        P(("grp", "sp", "tp"), None),
        P(),
        P("sp", "tp"),
        P("sp", None),
        P("sp", None),
        P(),
        P(),
        P("tp", "sp"),
    )
    out_specs = P(("grp", "sp", "tp"), None)
    return jax.shard_map(local, mesh=mesh, in_specs=in_specs, out_specs=out_specs, check_vma=False)
```

profile of v0, /device:TPU:33, one launch (start us, length us, event | category | flops | bytes accessed | tf_op | source)
XLA Modules:
  0.0 516.1 jit_solution(5865529478141150975)
XLA Ops:
  6.6 1.7 pad_maximum_fusion
  8.3 2.5 broadcast_in_dim.4
  10.9 44.9 %all-to-all-start = ((bf16[8,32,4096]{2,1,0:T(8,128)(2,1)}), bf16[8,32,4096]{2,1,0:T(8,128)(2,1)S(1)}, u32[]{:S(2)}, u32[]{:S(2)}) async-start(bf16[8,32,4096]{2,1,0:T(8,128)(2,1)} %broadcast_in_dim.4), calls=%async_computation | async-start | bytes 4194304 | tf_op jit(solution)/shard_map/all_to_all | solution.py:24
  55.8 26.3 %all-to-all-done = bf16[8,32,4096]{2,1,0:T(8,128)(2,1)S(1)} async-done(((bf16[8,32,4096]{2,1,0:T(8,128)(2,1)}), bf16[8,32,4096]{2,1,0:T(8,128)(2,1)S(1)}, u32[]{:S(2)}, u32[]{:S(2)}) %all-to-all-start) | async-done | bytes 2097184 | tf_op jit(solution)/shard_map/all_to_all | solution.py:24
  82.1 0.5 multiply_reduce_fusion
  82.6 0.1 rsqrt.28
  82.7 2.0 fusion.9
  84.7 90.2 %all-gather.4.cloned.1.call-done = bf16[4096,1280]{1,0:T(8,128)(2,1)} async-done(((bf16[128,1280]{1,0:T(8,128)(2,1)}), bf16[4096,1280]{1,0:T(8,128)(2,1)}) %all-gather.4.cloned.1.call-update) | async-done | bytes 10485776 | tf_op jit(solution)/shard_map/all_gather | solution.py:19
  174.9 3.8 fusion.72
  178.7 0.9 convolution_convert_fusion.2
  179.6 0.9 convolution_convert_fusion.1
  180.4 0.7 pad_maximum_fusion.1
  181.2 0.1 all-gather.8.cloned.1.call-start
  181.2 0.7 all-gather.8.cloned.1.call-update
  182.0 1.0 multiply_cosine_fusion.3
  183.0 2.5 multiply_reduce_fusion.1
  185.6 0.1 copy.11
  185.7 0.1 multiply_multiply_fusion
  185.8 0.3 multiply_subtract_fusion.1
  186.1 0.3 fusion.56
  186.4 133.9 %all-gather.6.cloned.1.call-done = bf16[8192,256]{0,1:T(8,128)(2,1)} async-done(((bf16[256,256]{0,1:T(8,128)(2,1)}), bf16[8192,256]{0,1:T(8,128)(2,1)}) %all-gather.6.cloned.1.call-update) | async-done | bytes 4194320 | tf_op jit(solution)/shard_map/all_gather | solution.py:19
  320.3 2.1 fusion.5
  322.4 2.1 fusion.7
  324.6 8.2 %fusion.53 = (bf16[8192,32]{0,1:T(8,128)(2,1)S(1)}, bf16[8192,32]{0,1:T(8,128)(2,1)S(1)}, bf16[8192,32]{0,1:T(8,128)(2,1)S(1)}, bf16[8192,32]{0,1:T(8,128)(2,1)S(1)}) fusion(f32[8192,1,128]{0,2,1:T(8,128)S(1)} %fusion.7, f32[32]{0:T(128)S(1)} %multiply_power_fusion, f32[8192]{0:T(1024)S(1)} %get-tuple-element.31, f32[8192]{0:T(1024)S(1)} %get-tuple-element.32), kind=kLoop, calls=%fused_computation.54 | loop fusion | flops 4718592 | bytes 6357120 | tf_op jit(solution)/shard_map/concatenate | solution.py:73
  332.8 7.1 %fusion.73 = (f32[512]{0:T(512)S(1)}, f32[512,8192]{1,0:T(8,128)}) fusion(bf16[512,128]{1,0:T(8,128)(2,1)S(1)} %bitcast.34, bf16[8192,32]{0,1:T(8,128)(2,1)S(1)} %get-tuple-element.11, bf16[8192,32]{0,1:T(8,128)(2,1)S(1)} %get-tuple-element.12, bf16[8192,32]{0,1:T(8,128)(2,1)S(1)} %get-tuple-element.8, bf16[8192,32]{0,1:T(8,128)(2,1)S(1)} %get-tuple-element.7), kind=kOutput, calls=%fused_computation.103 | convolution fusion | flops 1086324224 | bytes 19007488 | tf_op jit(solution)/shard_map/dot_general | solution.py:116
  339.9 8.3 %fusion = f32[512]{0:T(512)S(1)} fusion(f32[512,8192]{1,0:T(8,128)} %get-tuple-element.28, f32[512]{0:T(512)S(1)} %broadcast_maximum_fusion), kind=kLoop, calls=%fused_computation.1 | loop fusion | flops 8388096 | bytes 16781312 | tf_op jit(solution)/shard_map/reduce_sum | solution.py:124
  348.1 8.3 %fusion.37 = bf16[512,128]{1,0:T(8,128)(2,1)S(1)} fusion(bf16[8192,256]{0,1:T(8,128)(2,1)S(1)} %copy-done.1, f32[512,8192]{1,0:T(8,128)} %get-tuple-element.28, f32[512]{0:T(512)S(1)} %broadcast_maximum_fusion, f32[512]{0:T(512)S(1)} %fusion), kind=kOutput, calls=%fused_computation.42 | convolution fusion | flops 1082261504 | bytes 19009536 | tf_op jit(solution)/shard_map/dot_general | solution.py:125
  356.4 0.1 copy.12
  356.5 94.7 %all-gather.8.cloned.1.call-done = bf16[256,4096]{1,0:T(8,128)(2,1)} async-done(((bf16[256,128]{1,0:T(8,128)(2,1)}), bf16[256,4096]{1,0:T(8,128)(2,1)}) %all-gather.8.cloned.1.call-update) | async-done | bytes 2097168 | tf_op jit(solution)/shard_map/all_gather | solution.py:131
  451.3 2.3 convolution_convert_fusion
  453.6 54.9 %all_to_all.10 = bf16[8,32,4096]{2,1,0:T(8,128)(2,1)S(1)} all-to-all(bf16[8,32,4096]{2,1,0:T(8,128)(2,1)S(1)} %bitcast.33), channel_id=1, replica_groups=mesh['grp'=2,'sp'=32,'tp'=8] {'tp'}, dimensions={0} | all-to-all | bytes 4194304 | tf_op jit(solution)/shard_map/all_to_all | solution.py:45
  508.5 1.1 reduce_sum.52
  (21 shorter events, 0.2 us)
Async XLA Ops:
  6.5 168.3 %all-gather.4.cloned.1.call-start = ((), (), s32[]{:S(2)}) async-start(), calls=%async_computation.2 | async-start | bytes 10813440 | tf_op jit(solution)/shard_map/all_gather | solution.py:19
  8.3 74.4 %copy-start.2 = (f32[4096]{0:T(1024)S(1)}, f32[4096]{0:T(1024)}, u32[]{:S(2)}) copy-start(f32[4096]{0:T(1024)} %param.9) | copy-start | bytes 49156
  10.9 71.2 %all-to-all-start = ((bf16[8,32,4096]{2,1,0:T(8,128)(2,1)}), bf16[8,32,4096]{2,1,0:T(8,128)(2,1)S(1)}, u32[]{:S(2)}, u32[]{:S(2)}) async-start(bf16[8,32,4096]{2,1,0:T(8,128)(2,1)} %broadcast_in_dim.4), calls=%async_computation | async-start | bytes 4194304 | tf_op jit(solution)/shard_map/all_to_all | solution.py:24
  55.8 264.5 %all-gather.6.cloned.1.call-start = ((), (), s32[]{:S(2)}) async-start(), calls=%async_computation.3 | async-start | bytes 4325376 | tf_op jit(solution)/shard_map/all_gather | solution.py:19
  84.7 94.0 %copy-start = (bf16[256,4096]{1,0:T(8,128)(2,1)S(1)}, bf16[256,4096]{1,0:T(8,128)(2,1)}, u32[]{:S(2)}) copy-start(bf16[256,4096]{1,0:T(8,128)(2,1)} %fusion.9) | copy-start | bytes 6291460
  179.6 6.1 %copy-start.3 = (f32[128]{0:T(128)S(1)}, f32[128]{0:T(128)}, u32[]{:S(2)}) copy-start(f32[128]{0:T(128)} %param.13) | copy-start | bytes 1540
  181.2 270.1 %all-gather.8.cloned.1.call-start = ((), (), s32[]{:S(2)}) async-start(), calls=%async_computation.4 | async-start | bytes 2162688 | tf_op jit(solution)/shard_map/all_gather | solution.py:131
  185.5 136.9 %copy-start.4 = (f32[128]{0:T(128)S(1)}, f32[128]{0:T(128)}, u32[]{:S(2)}) copy-start(f32[128]{0:T(128)} %param.14) | copy-start | bytes 1540
  339.9 8.3 %copy-start.1 = (bf16[8192,256]{0,1:T(8,128)(2,1)S(1)}, bf16[8192,256]{0,1:T(8,128)(2,1)}, u32[]{:S(2)}) copy-start(bf16[8192,256]{0,1:T(8,128)(2,1)} %all-gather.6.cloned.1.call-done) | copy-start | bytes 12582916
Sparse Core Ops, SparseCore 0:
  9.4 165.4 all-gather.3
  181.3 138.9 all-gather.5
  322.3 128.8 all-gather.7
where the time goes:
time: 517 us; the launch traced here: 516 us
  waiting for transfers between devices  346 us (67%)
  blocking collectives  54.9 us (11%)
  starting transfers between devices  45 us (9%)
  other arithmetic  28.3 us (5%)
  matrix products  21.9 us (4%)
  between operations  13.3 us (3%)
  local copies, waits for them, and re-layouts  6.66 us (1%)
    all_gather x2, waiting for transfers between devices, sent_together(): lax.all_gather(both, axis, axis=dim, tiled=True)  224 us
    all_gather x1, waiting for transfers between devices, local(): full_out = lax.all_gather(w_out, 'sp', axis=1, tiled=True)  94.7 us
    all_to_all x1, blocking collectives, sent_and_summed(): lax.all_to_all(pieces, axis, split_axis=0, concat_axis=0, tiled=True)  54.9 us
    all_to_all x1, starting transfers between devices, sent_to_all(): return lax.all_to_all(copies, axis, split_axis=0, concat_axis=0, tiled=True)  44.9 us
    all_to_all x1, waiting for transfers between devices, sent_to_all(): return lax.all_to_all(copies, axis, split_axis=0, concat_axis=0, tiled=True)  26.3 us
  transfers between devices with their start and end apart: 4, of which 4 were waited for; matrix products, arithmetic and copies ran while one was open for 9% of the time, Pallas kernels for 0%

commit v1 on v0

v1 whole, which is shorter than its diff:
```python
import functools

import jax
import jax.numpy as jnp
from jax import lax
from jax.experimental import pallas as pl
from jax.experimental.pallas import tpu as pltpu
from jax.sharding import PartitionSpec as P

HEAD = 128
GRID_W = 64
EPS = 1e-06
CHUNKS = 2
QUARTERS = 4
MESH = pl.DeviceIdType.MESH


def remote(src, dst, send_sem, recv_sem, device):
    return pltpu.make_async_remote_copy(
        src_ref=src, dst_ref=dst, send_sem=send_sem, recv_sem=recv_sem, device_id=device, device_id_type=MESH
    )


def fused(
    sizes,
    tok_hbm,
    gain_ref,
    wq_hbm,
    wk_hbm,
    wv_hbm,
    qg_ref,
    kg_ref,
    wo_hbm,
    inv_ref,
    out_ref,
    tok,
    normed,
    wa,
    wo,
    kv,
    cosine,
    sine,
    queries,
    peak,
    total,
    summed,
    terms,
    partner_terms,
    pair_sums,
    arrived,
    in_sems,
    nx_ss,
    nx_rs,
    nd_ss,
    nd_rs,
    wa_ss,
    wa_rs,
    wy_ss,
    wy_rs,
    kv_ss,
    kv_rs,
    kd_ss,
    kd_rs,
    wo_ss,
    wo_rs,
    td_ss,
    td_rs,
    x_ss,
    x_rs,
):
    n, n_tp = sizes
    chips = n_tp // 2
    hops = n // 2
    grp, z, t = lax.axis_index("grp"), lax.axis_index("sp"), lax.axis_index("tp")
    x, core = t // 2, t % 2
    half = grp % 2
    right, left = {"sp": lax.rem(z + 1, n)}, {"sp": lax.rem(z + n - 1, n)}
    mate = {"tp": t + 1 - 2 * core}
    twin = {"grp": grp + 1 - 2 * half}
    across = [{"tp": lax.rem(t + 2 * d, n_tp)} for d in range(1, chips)]

    own_rows, width = tok.shape
    rows = own_rows * n_tp
    depth = wa.shape[1]
    q_cols = wa.shape[2] - HEAD
    heads = q_cols // HEAD
    half_depth = depth // 2
    out_rows = wo.shape[1]
    half_out = out_rows // 2

    loads = [
        pltpu.make_async_copy(wq_hbm, wa.at[z, :, pl.ds(0, q_cols)], in_sems.at[0]),
        pltpu.make_async_copy(wo_hbm, wo.at[z], in_sems.at[2]),
        pltpu.make_async_copy(tok_hbm, tok, in_sems.at[3]),
    ]
    for load in loads:
        load.start()
    columns = pl.ds(pl.multiple_of(x * HEAD, HEAD), HEAD)

    @pl.when(core == 0)
    def _():
        pltpu.make_async_copy(wk_hbm.at[:, columns], wa.at[z, :, pl.ds(q_cols, HEAD)], in_sems.at[1]).start()

    @pl.when(core == 1)
    def _():
        pltpu.make_async_copy(wv_hbm.at[:, columns], wa.at[z, :, pl.ds(q_cols, HEAD)], in_sems.at[1]).start()

    barrier = pltpu.get_barrier_semaphore()
    peers = [right, left, mate, twin] + across
    for peer in peers:
        pl.semaphore_signal(barrier, inc=1, device_id=peer, device_id_type=MESH)
    pl.semaphore_wait(barrier, len(peers))

    def back(s):
        return lax.rem(z - s + n, n)

    def ahead(s):
        return lax.rem(z + s, n)

    piece_rows = half_depth // CHUNKS

    def wa_ring(way, slot, s, c):
        first = pl.multiple_of(half * half_depth + c * piece_rows, piece_rows)
        piece = wa.at[slot, pl.ds(first, piece_rows), :]
        return remote(piece, piece, wa_ss.at[way], wa_rs.at[way, s, c], right if way == 0 else left)

    def wa_twin(slot):
        piece = wa.at[slot, pl.ds(pl.multiple_of(half * half_depth, half_depth), half_depth), :]
        return remote(piece, piece, wy_ss.at[0], wy_rs.at[0], twin)

    def wo_ring(way, slot, s):
        piece = wo.at[slot, pl.ds(pl.multiple_of(half * half_out, half_out), half_out), :]
        return remote(piece, piece, wo_ss.at[way], wo_rs.at[way, s], right if way == 0 else left)

    def wo_twin(slot):
        piece = wo.at[slot, pl.ds(pl.multiple_of(half * half_out, half_out), half_out), :]
        return remote(piece, piece, wy_ss.at[1], wy_rs.at[1], twin)

    def kv_ring(way, slot, s, c):
        piece = kv.at[core, slot, pl.ds(c * (rows // CHUNKS), rows // CHUNKS), :]
        return remote(piece, piece, kv_ss.at[way], kv_rs.at[way, s, c], right if way == 0 else left)

    def kv_mate(way, slot, s, c):
        piece = kv.at[core, slot, pl.ds(c * (rows // CHUNKS), rows // CHUNKS), :]
        return remote(piece, piece, kd_ss.at[0], kd_rs.at[way, s], mate)

    def kv_from_mate(way, slot, s):
        block = kv.at[1 - core, slot]
        return remote(block, block, kd_ss.at[0], kd_rs.at[way, s], mate)

    loads[0].wait()
    pltpu.make_async_copy(wk_hbm.at[:, columns], wa.at[z, :, pl.ds(q_cols, HEAD)], in_sems.at[1]).wait()
    for c in range(CHUNKS):
        wa_ring(0, z, 0, c).start()
        wa_ring(1, z, 0, c).start()

    loads[2].wait()
    floats = tok[...].astype(jnp.float32)
    scale = lax.rsqrt(jnp.mean(floats * floats, axis=-1, keepdims=True) + EPS)
    normed[t] = (floats * scale * gain_ref[...]).astype(jnp.bfloat16)

    def normed_to(d):
        return remote(normed.at[t], normed.at[t], nx_ss.at[d - 1], nx_rs.at[d - 1], across[d - 1])

    def normed_mate(d):
        slot = lax.rem(t + n_tp - 2 * d, n_tp)
        return remote(normed.at[slot], normed.at[slot], nd_ss.at[d], nd_rs.at[d], mate)

    def normed_from(d):
        slot = lax.rem(t + n_tp - 2 * d, n_tp)
        return remote(normed.at[slot], normed.at[slot], nx_ss.at[d - 1], nx_rs.at[d - 1], across[d - 1])

    def normed_from_mate(d):
        slot = lax.rem(t + 1 - 2 * core + n_tp - 2 * d, n_tp)
        return remote(normed.at[slot], normed.at[slot], nd_ss.at[d], nd_rs.at[d], mate)

    for d in range(1, chips):
        normed_to(d).start()
    normed_mate(0).start()

    lane = lax.broadcasted_iota(jnp.int32, (rows, HEAD), 1)
    place = lax.broadcasted_iota(jnp.int32, (rows, HEAD), 0) + z * rows
    spot = jnp.where(lane < HEAD // 2, place // GRID_W, place % GRID_W).astype(jnp.float32)
    angles = spot * inv_ref[...]
    first_half = lane % (HEAD // 2) < HEAD // 4
    cosine[...] = jnp.cos(angles)
    sine[...] = jnp.where(first_half, -jnp.sin(angles), jnp.sin(angles))

    def turned(raw, gain):
        heads_in = raw.astype(jnp.bfloat16).astype(jnp.float32)
        scale = lax.rsqrt(jnp.mean(heads_in * heads_in, axis=-1, keepdims=True) + EPS)
        scaled = heads_in * scale * gain
        lanes = lax.broadcasted_iota(jnp.int32, scaled.shape, 1)
        other = jnp.where(
            lanes % (HEAD // 2) < HEAD // 4,
            pltpu.roll(scaled, HEAD - HEAD // 4, 1),
            pltpu.roll(scaled, HEAD // 4, 1),
        )
        return scaled * cosine[...] + other * sine[...]

    def wa_step(s, carry):
        for c in range(CHUNKS):
            wa_ring(0, back(s), s - 1, c).wait_recv()
            wa_ring(0, back(s), s, c).start()
            wa_ring(1, ahead(s), s - 1, c).wait_recv()

            @pl.when(s < hops - 1)
            def _():
                wa_ring(1, ahead(s), s, c).start()

        wa_twin(back(s)).start()
        wa_twin(ahead(s)).start()
        return carry

    split = hops - 4
    lax.fori_loop(1, split, wa_step, 0)
    for d in range(1, chips):
        normed_from(d).wait_recv()
        normed_mate(d).start()
    lax.fori_loop(split, hops, wa_step, 0)
    for c in range(CHUNKS):
        wa_ring(0, back(hops), hops - 1, c).wait_recv()
    wa_twin(back(hops)).start()
    for d in range(chips):
        normed_from_mate(d).wait_recv()
    incoming = wa.at[pl.ds(0, n - 1), pl.ds(0, half_depth), :]
    remote(incoming, incoming, wy_ss.at[0], wy_rs.at[0], twin).wait_recv()

    tokens_in = normed[...].reshape(rows, width)
    projected = jnp.dot(
        tokens_in, wa[:, :, q_cols:].reshape(width, HEAD), preferred_element_type=jnp.float32
    )

    @pl.when(core == 0)
    def _():
        kv[0, z] = turned(projected, kg_ref[...]).astype(jnp.bfloat16)

    @pl.when(core == 1)
    def _():
        kv[1, z] = projected.astype(jnp.bfloat16)

    loads[1].wait()
    for c in range(CHUNKS):
        kv_ring(0, z, 0, c).start()
        kv_ring(1, z, 0, c).start()
    for c in range(CHUNKS):
        kv_mate(0, z, 0, c).start()
    wo_ring(0, z, 0).start()
    wo_ring(1, z, 0).start()

    for h in range(heads):
        raw = jnp.dot(
            normed[...].reshape(rows, width),
            wa[:, :, h * HEAD : (h + 1) * HEAD].reshape(width, HEAD),
            preferred_element_type=jnp.float32,
        )
        queries[h] = (turned(raw, qg_ref[...]) * HEAD ** (-0.5)).astype(jnp.bfloat16)

    peak[...] = jnp.full_like(peak, -1e30)
    total[...] = jnp.zeros_like(total)
    summed[...] = jnp.zeros_like(summed)

    def attend(a, b):
        for h in range(heads):
            q = queries[h]
            scores = [
                lax.dot_general(q, kv[0, i], (((1,), (1,)), ((), ())), preferred_element_type=jnp.float32)
                for i in (a, b)
            ]
            old = peak[h]
            new = jnp.maximum(old, jnp.max(jnp.maximum(*scores), axis=1, keepdims=True))
            fade = jnp.exp(old - new)
            wide = jnp.concatenate([new] * (rows // HEAD), axis=1)
            weights = [jnp.exp(part - wide) for part in scores]
            peak[h] = new
            total[h] = fade * total[h] + jnp.sum(weights[0] + weights[1], axis=1, keepdims=True)
            summed[h] = (
                fade * summed[h]
                + jnp.dot(weights[0].astype(jnp.bfloat16), kv[1, a], preferred_element_type=jnp.float32)
                + jnp.dot(weights[1].astype(jnp.bfloat16), kv[1, b], preferred_element_type=jnp.float32)
            )

    def kv_step(s, carry):
        for c in range(CHUNKS):
            kv_ring(0, back(s), s - 1, c).wait_recv()
            kv_ring(0, back(s), s, c).start()
            kv_mate(0, back(s), s, c).start()
            kv_ring(1, ahead(s), s - 1, c).wait_recv()

            @pl.when(s < hops - 1)
            def _():
                kv_ring(1, ahead(s), s, c).start()

            kv_mate(1, ahead(s), s, c).start()
        wo_ring(0, back(s), s - 1).wait_recv()
        wo_ring(0, back(s), s).start()
        wo_twin(back(s)).start()
        wo_ring(1, ahead(s), s - 1).wait_recv()

        @pl.when(s < hops - 1)
        def _():
            wo_ring(1, ahead(s), s).start()

        wo_twin(ahead(s)).start()

        @pl.when(s > 1)
        def _():
            kv_from_mate(0, back(s - 1), s - 1).wait_recv()
            kv_from_mate(1, ahead(s - 1), s - 1).wait_recv()
            attend(back(s - 1), ahead(s - 1))

        return carry

    lax.fori_loop(1, hops, kv_step, 0)
    for c in range(CHUNKS):
        kv_ring(0, back(hops), hops - 1, c).wait_recv()
        kv_mate(0, back(hops), hops, c).start()
    wo_ring(0, back(hops), hops - 1).wait_recv()
    wo_twin(back(hops)).start()
    kv_from_mate(0, back(hops - 1), hops - 1).wait_recv()
    kv_from_mate(1, ahead(hops - 1), hops - 1).wait_recv()
    attend(back(hops - 1), ahead(hops - 1))
    kv_from_mate(0, z, 0).wait_recv()
    kv_from_mate(0, back(hops), hops).wait_recv()
    attend(z, back(hops))

    attended = jnp.concatenate([(summed[h] / total[h]).astype(jnp.bfloat16) for h in range(heads)], axis=1)

    incoming = wo.at[pl.ds(0, n - 1), pl.ds(0, half_out), :]
    remote(incoming, incoming, wy_ss.at[1], wy_rs.at[1], twin).wait_recv()

    per_piece = n // QUARTERS
    cols = wo.shape[2]

    def term_mate(p):
        return remote(terms.at[p, 1 - core], partner_terms.at[p], td_ss.at[p], td_rs.at[p], mate)

    def project(p, carry):
        for j in range(per_piece // 2):
            both = jnp.concatenate([wo[p * per_piece + 2 * j], wo[p * per_piece + 2 * j + 1]], axis=1)
            term = jnp.dot(attended, both, preferred_element_type=jnp.float32).astype(jnp.bfloat16)
            for owner in range(n_tp):
                terms[p, owner % 2, owner // 2, :, 2 * j * cols : (2 * j + 2) * cols] = term[
                    owner * own_rows : (owner + 1) * own_rows
                ]
        term_mate(p).start()
        return carry

    lax.fori_loop(0, QUARTERS, project, 0)

    def sum_to(p, d):
        there = lax.rem(x + d, chips)
        return remote(
            pair_sums.at[p, there], arrived.at[p, d - 1], x_ss.at[p, d - 1], x_rs.at[p, d - 1], across[d - 1]
        )

    far_first = sorted(range(1, chips), key=lambda d: -min(d, chips - d))

    def exchange(p, carry):
        term_mate(p).wait_recv()
        pair_sums[p] = (
            terms[p, core].astype(jnp.float32) + partner_terms[p].astype(jnp.float32)
        ).astype(jnp.bfloat16)
        for d in far_first:
            sum_to(p, d).start()
        return carry

    lax.fori_loop(0, QUARTERS, exchange, 0)
    piece_cols = per_piece * cols
    for p in range(QUARTERS):
        mixed = terms[p, core, x].astype(jnp.float32) + partner_terms[p, x].astype(jnp.float32)
        for d in range(1, chips):
            sum_to(p, d).wait_recv()
            mixed = mixed + arrived[p, d - 1].astype(jnp.float32)
        out_ref[:, p * piece_cols : (p + 1) * piece_cols] = mixed.astype(out_ref.dtype)

    for d in range(1, chips):
        normed_to(d).wait_send()
    for d in range(chips):
        normed_mate(d).wait_send()
    for way, count in ((0, hops), (1, hops - 1)):
        sent = wa.at[pl.ds(0, count), pl.ds(0, half_depth), :]
        remote(sent, sent, wa_ss.at[way], wa_rs.at[way, 0, 0], right).wait_send()
        sent = wo.at[pl.ds(0, count), pl.ds(0, half_out), :]
        remote(sent, sent, wo_ss.at[way], wo_rs.at[way, 0], right).wait_send()
        sent = kv.at[0, pl.ds(0, count)]
        remote(sent, sent, kv_ss.at[way], kv_rs.at[way, 0, 0], right).wait_send()
    sent = wa.at[pl.ds(0, n - 1), pl.ds(0, half_depth), :]
    remote(sent, sent, wy_ss.at[0], wy_rs.at[0], twin).wait_send()
    sent = wo.at[pl.ds(0, n - 1), pl.ds(0, half_out), :]
    remote(sent, sent, wy_ss.at[1], wy_rs.at[1], twin).wait_send()
    remote(kv.at[0], kv.at[0], kd_ss.at[0], kd_rs.at[0, 0], mate).wait_send()
    for p in range(QUARTERS):
        term_mate(p).wait_send()
        for d in range(1, chips):
            sum_to(p, d).wait_send()


def solution(mesh):
    n, n_tp = mesh.shape["sp"], mesh.shape["tp"]

    def local(tokens, input_gain, w_query, w_key, w_value, query_gain, key_gain, w_out):
        own_rows, width = tokens.shape
        rows = own_rows * n_tp
        depth, q_cols = w_query.shape
        heads = q_cols // HEAD
        out_rows, cols = w_out.shape
        chips = n_tp // 2
        hops = n // 2
        piece_cols = width // QUARTERS
        quarter = HEAD // 4
        inverse = 10000.0 ** (-jnp.arange(quarter, dtype=jnp.float32) * 2.0 / (2 * quarter))
        inverse = jnp.tile(inverse, 4)[None, :]
        bf16, f32 = jnp.bfloat16, jnp.float32
        dma = pltpu.SemaphoreType.DMA
        any_spec = pl.BlockSpec(memory_space=pl.ANY)
        vmem_spec = pl.BlockSpec(memory_space=pltpu.VMEM)
        return pl.pallas_call(
            functools.partial(fused, (n, n_tp)),
            out_shape=jax.ShapeDtypeStruct((own_rows, width), bf16),
            in_specs=[
                any_spec,
                vmem_spec,
                any_spec,
                any_spec,
                any_spec,
                vmem_spec,
                vmem_spec,
                any_spec,
                vmem_spec,
            ],
            out_specs=vmem_spec,
            scratch_shapes=[
                pltpu.VMEM((own_rows, width), bf16),
                pltpu.VMEM((n_tp, own_rows, width), bf16),
                pltpu.VMEM((n, depth, q_cols + HEAD), bf16),
                pltpu.VMEM((n, out_rows, cols), bf16),
                pltpu.VMEM((2, n, rows, HEAD), bf16),
                pltpu.VMEM((rows, HEAD), f32),
                pltpu.VMEM((rows, HEAD), f32),
                pltpu.VMEM((heads, rows, HEAD), bf16),
                pltpu.VMEM((heads, rows, HEAD), f32),
                pltpu.VMEM((heads, rows, HEAD), f32),
                pltpu.VMEM((heads, rows, HEAD), f32),
                pltpu.VMEM((QUARTERS, 2, chips, own_rows, piece_cols), bf16),
                pltpu.VMEM((QUARTERS, chips, own_rows, piece_cols), bf16),
                pltpu.VMEM((QUARTERS, chips, own_rows, piece_cols), bf16),
                pltpu.VMEM((QUARTERS, chips - 1, own_rows, piece_cols), bf16),
                dma((4,)),
                dma((chips - 1,)),
                dma((chips - 1,)),
                dma((chips,)),
                dma((chips,)),
                dma((2,)),
                dma((2, hops, CHUNKS)),
                dma((2,)),
                dma((2,)),
                dma((2,)),
                dma((2, hops, CHUNKS)),
                dma((1,)),
                dma((2, hops + 1)),
                dma((2,)),
                dma((2, hops)),
                dma((QUARTERS,)),
                dma((QUARTERS,)),
                dma((QUARTERS, chips - 1)),
                dma((QUARTERS, chips - 1)),
            ],
            compiler_params=pltpu.CompilerParams(
                collective_id=0, has_side_effects=True, vmem_limit_bytes=48 * 1024 * 1024
            ),
        )(
            tokens,
            input_gain[None, :],
            w_query,
            w_key,
            w_value,
            query_gain[None, :],
            key_gain[None, :],
            w_out,
            inverse,
        )

    in_specs = (
        P(("grp", "sp", "tp"), None),
        P(),
        P("sp", "tp"),
        P("sp", None),
        P("sp", None),
        P(),
        P(),
        P("tp", "sp"),
    )
    out_specs = P(("grp", "sp", "tp"), None)
    return jax.shard_map(local, mesh=mesh, in_specs=in_specs, out_specs=out_specs, check_vma=False)
```

time: 517 us -> 182 us (0.35)
  waiting for transfers between devices: 346 us -> 0 us
  Pallas kernels: 0 us -> 175 us
  blocking collectives: 54.9 us -> 0 us
  starting transfers between devices: 45 us -> 0 us
  other arithmetic: 28.3 us -> 0.01 us
  matrix products: 21.9 us -> 0 us
  between operations: 13.3 us -> 0.04 us
    all_gather x3 -> x0, waiting for transfers between devices: 319 us -> none  [the longest x2 224 us: sent_together(): lax.all_gather(both, axis, axis=dim, tiled=True)]
    pallas_call x0 -> x1, Pallas kernels: none -> 175 us  [local(): pl.pallas_call(functools.partial(fused, (n, n_tp)), out_shape=jax.ShapeDt...]
    all_to_all x1 -> x0, blocking collectives: 54.9 us -> none  [sent_and_summed(): lax.all_to_all(pieces, axis, split_axis=0, concat_axis=0, tiled=True)]
    all_to_all x1 -> x0, starting transfers between devices: 44.9 us -> none  [sent_to_all(): return lax.all_to_all(copies, axis, split_axis=0, concat_axis=0, tiled=True)]
    all_to_all x1 -> x0, waiting for transfers between devices: 26.3 us -> none  [sent_to_all(): return lax.all_to_all(copies, axis, split_axis=0, concat_axis=0, tiled=True)]
    dot_general x6 -> x0, matrix products: 21.9 us -> none  [the longest x1 8.26 us: local(): jnp.dot(weights.astype(jnp.bfloat16), piece[1], preferred_element_type=jn...]
    reduce_sum x4 -> x0, other arithmetic: 11.9 us -> none  [the longest x1 8.26 us: local(): total = jnp.sum(weights, axis=1)]
    concatenate x3 -> x0, other arithmetic: 10.6 us -> none  [the longest x1 8.25 us: turn_heads(): jnp.concatenate([rotate_half(row_part, row_angle), rotate_half(col_part,...]
  transfers between devices with their start and end apart: 4 -> 0, of which waited for: 4 -> 0; matrix products, arithmetic and copies ran while one was open for 9% -> 0% of each run, Pallas kernels for 0% -> 0%
where the time goes in v1:
time: 182 us
  Pallas kernels  175 us (96%)
  local copies, waits for them, and re-layouts  6.52 us (4%)
    pallas_call x1, Pallas kernels, local(): pl.pallas_call(functools.partial(fused, (n, n_tp)), out_shape=jax.ShapeDt...  175 us
    unnamed x17, local copies, waits for them, and re-layouts  6.43 us

profile of v1, /device:TPU:33, one launch (start us, length us, event | category | flops | bytes accessed | tf_op | source)
XLA Modules:
  0.0 181.7 jit_solution(3750433390657692408)
XLA Ops:
  0.0 0.0 copy-start.6
  0.0 0.0 copy-start.7
  0.0 0.1 broadcast_in_dim_tile.3.inv_ref
  0.1 0.6 copy-done.6
  0.7 0.0 copy-done.7
  0.7 0.0 copy-start
  0.7 0.9 copy-done
  1.6 0.0 copy-start.1
  1.6 0.9 copy-done.1
  2.6 0.0 copy-start.2
  2.6 0.9 copy-done.2
  3.5 0.0 copy-start.3
  3.5 0.8 copy-done.3
  4.3 0.0 copy-start.4
  4.3 0.8 copy-done.4
  5.1 0.0 copy-start.5
  5.1 0.7 copy-done.5
  5.9 175.2 %shard_map.82 = bf16[32,4096]{1,0:T(8,128)(2,1)S(1)} custom-call(bf16[32,4096]{1,0:T(8,128)(2,1)S(1)} %copy-done, f32[1,4096]{1,0:T(1,128)S(1)} %bitcast.3, bf16[128,256]{1,0:T(8,128)(2,1)S(1)} %copy-done.3, bf16[128,512]{1,0:T(8,128)(2,1)S(1)} %copy-done.1, bf16[128,512]{1,0:T(8,128)(2,1)S(1)} %copy-done.2, f32[1,128]{1,0:T(1,128)S(1)} %bitcast.4, ...), custom_call_target="tpu_custom_call" | custom-call | tf_op jit(solution)/shard_map/pallas_call | solution.py:418
  181.0 0.7 copy.10
  (2 shorter events, 0.0 us)
Async XLA Ops:
  0.0 0.7 copy-start.6
  0.0 0.7 copy-start.7
  0.7 0.9 copy-start
  1.6 0.9 copy-start.1
  2.6 0.9 copy-start.2
  3.5 0.8 copy-start.3
  4.3 0.8 copy-start.4
  5.1 0.7 copy-start.5

commit v2 on v1

v2 whole, which is shorter than its diff:
```python
import functools

import jax
import jax.numpy as jnp
import numpy as np
from jax import lax
from jax.experimental import pallas as pl
from jax.experimental.pallas import tpu as pltpu
from jax.sharding import PartitionSpec as P

HEAD = 128
GRID_W = 64
EPS = 1e-06
CHUNKS = 4
FAR = 4
MID = 2
LEAD = 6
QUARTERS = 4
MESH = pl.DeviceIdType.MESH


def remote(src, dst, send_sem, recv_sem, device):
    return pltpu.make_async_remote_copy(
        src_ref=src, dst_ref=dst, send_sem=send_sem, recv_sem=recv_sem, device_id=device, device_id_type=MESH
    )


def fused(
    sizes,
    tok_hbm,
    gain_hbm,
    wq_hbm,
    wk_hbm,
    wv_hbm,
    qg_hbm,
    kg_hbm,
    wo_hbm,
    inv_hbm,
    out_hbm,
    mixed,
    tok,
    gain,
    qg,
    kg,
    inv,
    normed,
    wkv,
    wq,
    wo,
    kv,
    cosine,
    sine,
    queries,
    peak,
    total,
    summed,
    terms,
    partner_terms,
    pair_sums,
    relayed,
    arrived,
    in_sems,
    out_sems,
    nx_ss,
    nx_rs,
    nd_ss,
    nd_rs,
    wkv_ss,
    wkv_rs,
    w_ss,
    w_rs,
    twin_ss,
    twin_rs,
    md_ss,
    md_rs,
    kv_ss,
    kv_rs,
    kd_ss,
    kd_rs,
    td_ss,
    td_rs,
    x_ss,
    x_rs,
):
    n, n_tp = sizes
    chips = n_tp // 2
    hops = n // 2
    grp, z, t = lax.axis_index("grp"), lax.axis_index("sp"), lax.axis_index("tp")
    x, core = t // 2, t % 2
    half = grp % 2
    other_t = t + 1 - 2 * core
    low_t = t - core
    mate = {"tp": other_t}
    other_grp = grp + 1 - 2 * half
    across = [{"tp": lax.rem(t + 2 * d, n_tp)} for d in range(1, chips)]

    own_rows, width = tok.shape
    rows = own_rows * n_tp
    q_cols = wq.shape[3]
    heads = q_cols // HEAD
    cols = wo.shape[3]

    def back(s):
        return lax.rem(z - s + n, n)

    def ahead(s):
        return lax.rem(z + s, n)

    def toward(way, j):
        return ahead(j) if way == 0 else back(j)

    def source(way, d):
        return back(d) if way == 0 else ahead(d)

    columns = pl.ds(pl.multiple_of(x * HEAD, HEAD), HEAD)
    loads = [
        pltpu.make_async_copy(source_ref, target, in_sems.at[i])
        for i, (source_ref, target) in enumerate(
            (
                (wk_hbm.at[:, columns], wkv.at[z, :, pl.ds(0, HEAD)]),
                (wv_hbm.at[:, columns], wkv.at[z, :, pl.ds(HEAD, HEAD)]),
                (tok_hbm, tok),
                (gain_hbm, gain),
                (wq_hbm, wq.at[z, core]),
                (wo_hbm, wo.at[z, core]),
                (qg_hbm, qg),
                (kg_hbm, kg),
                (inv_hbm, inv),
            )
        )
    ]
    for load in loads:
        load.start()

    peers = [mate, {"grp": other_grp}, {"grp": other_grp, "tp": other_t}] + across
    peers += [{"sp": toward(way, j)} for way in (0, 1) for j in range(1, FAR + 1)]
    peers += [{"sp": toward(way, j), "tp": other_t} for way in (0, 1) for j in range(1, MID + 1)]
    barrier = pltpu.get_barrier_semaphore()
    for peer in peers:
        pl.semaphore_signal(barrier, inc=1, device_id=peer, device_id_type=MESH)
    pl.semaphore_wait(barrier, len(peers))

    wkv_half = wkv.shape[1] // 2

    def wkv_piece(slot):
        return wkv.at[slot, pl.ds(pl.multiple_of(half * wkv_half, wkv_half), wkv_half), :]

    def wkv_ring(way, d, j):
        piece = wkv_piece(source(way, d))
        return remote(piece, piece, wkv_ss.at[way], wkv_rs.at[way, d // FAR, j - 1], {"sp": toward(way, j)})

    def wkv_arrival(way, d):
        piece = wkv_piece(source(way, d))
        return remote(
            piece, piece, wkv_ss.at[way], wkv_rs.at[way, (d - 1) // FAR, (d - 1) % FAR], {"sp": toward(way, 1)}
        )

    def wkv_twin(way, d):
        piece = wkv_piece(source(way, d))
        return remote(piece, piece, twin_ss.at[2], twin_rs.at[2], {"grp": other_grp})

    reach = (hops, hops - 1)

    def wkv_send(way, d):
        for j in [FAR] + list(range(1, FAR)):
            if d + j <= reach[way]:
                wkv_ring(way, d, j).start()

    weights = (wq, wo)

    def half_rows(f):
        size = weights[f].shape[2] // 2
        return pl.ds(pl.multiple_of(half * size, size), size)

    def w_piece(f, slot):
        return weights[f].at[slot, :, half_rows(f), :]

    def w_own(f, way, j):
        piece = weights[f].at[z, core, half_rows(f), :]
        return remote(piece, piece, w_ss.at[f], w_rs.at[f, way, 0, j - 1], {"sp": toward(way, j), "tp": low_t})

    def w_ring(f, way, k, j):
        piece = w_piece(f, source(way, MID * k))
        return remote(piece, piece, w_ss.at[f], w_rs.at[f, way, k, j - 1], {"sp": toward(way, j)})

    def w_arrival(f, way, k, j):
        piece = w_piece(f, source(way, MID * k + j))
        return remote(piece, piece, w_ss.at[f], w_rs.at[f, way, k, j - 1], {"sp": toward(way, 1)})

    def w_share(f, way, d):
        slot = source(way, d)
        for c in (0, 1):
            piece = weights[f].at[slot, c, half_rows(f), :]
            remote(piece, piece, twin_ss.at[f], twin_rs.at[f], {"grp": other_grp, "tp": low_t + c}).start()
        piece = weights[f].at[slot, 1, half_rows(f), :]
        remote(piece, piece, md_ss.at[f], md_rs.at[f], mate).start()

    def several(f, count, c=None):
        size = weights[f].shape[2] // 2
        if c is None:
            return weights[f].at[pl.ds(0, count), :, pl.ds(0, size), :]
        return weights[f].at[pl.ds(0, count), c, pl.ds(0, size), :]

    chunk = 2 * rows // CHUNKS

    def kv_piece(slot, c):
        return kv.at[slot, c * chunk // rows, pl.ds(c * chunk % rows, chunk), :]

    def kv_ring(way, slot, s, c):
        piece = kv_piece(slot, c)
        return remote(piece, piece, kv_ss.at[way], kv_rs.at[way, s, c], {"sp": toward(way, 1)})

    def kv_mate(way, slot, s, c):
        piece = kv_piece(slot, c)
        return remote(piece, piece, kd_ss.at[0], kd_rs.at[way, s], mate)

    def kv_from_mate(way, slot, s):
        return remote(kv.at[slot], kv.at[slot], kd_ss.at[0], kd_rs.at[way, s], mate)

    def normed_to(d):
        return remote(normed.at[t], normed.at[t], nx_ss.at[d - 1], nx_rs.at[d - 1], across[d - 1])

    def normed_slot(d, of):
        return normed.at[lax.rem(of + n_tp - 2 * d, n_tp)]

    def normed_mate(d):
        return remote(normed_slot(d, t), normed_slot(d, t), nd_ss.at[d], nd_rs.at[d], mate)

    def normed_from(d):
        return remote(normed_slot(d, t), normed_slot(d, t), nx_ss.at[d - 1], nx_rs.at[d - 1], across[d - 1])

    def normed_from_mate(d):
        return remote(normed_slot(d, other_t), normed_slot(d, other_t), nd_ss.at[d], nd_rs.at[d], mate)

    loads[0].wait()
    loads[1].wait()

    @pl.when(core == 1)
    def _():
        wkv_send(0, 0)
        wkv_send(1, 0)

    loads[2].wait()
    loads[3].wait()
    floats = tok[...].astype(jnp.float32)
    scale = lax.rsqrt(jnp.mean(floats * floats, axis=-1, keepdims=True) + EPS)
    normed[t] = (floats * scale * gain[...]).astype(jnp.bfloat16)
    for d in range(1, chips):
        normed_to(d).start()
    normed_mate(0).start()

    def w_own_sends(f):
        loads[4 + f].wait()
        for j in range(MID, 0, -1):
            for way in (0, 1):
                w_own(f, way, j).start()

    w_own_sends(0)
    for load in loads[6:]:
        load.wait()

    lane = lax.broadcasted_iota(jnp.int32, (rows, HEAD), 1)
    place = lax.broadcasted_iota(jnp.int32, (rows, HEAD), 0) + z * rows
    spot = jnp.where(lane < HEAD // 2, place // GRID_W, place % GRID_W).astype(jnp.float32)
    angles = spot * inv[...]
    first_half = lane % (HEAD // 2) < HEAD // 4
    cosine[...] = jnp.cos(angles)
    sine[...] = jnp.where(first_half, -jnp.sin(angles), jnp.sin(angles))
    peak[...] = jnp.full_like(peak, -1e30)
    total[...] = jnp.zeros_like(total)
    summed[...] = jnp.zeros_like(summed)

    def turned(raw, head_gain):
        heads_in = raw.astype(jnp.bfloat16).astype(jnp.float32)
        scale = lax.rsqrt(jnp.mean(heads_in * heads_in, axis=-1, keepdims=True) + EPS)
        scaled = heads_in * scale * head_gain
        lanes = lax.broadcasted_iota(jnp.int32, scaled.shape, 1)
        other = jnp.where(
            lanes % (HEAD // 2) < HEAD // 4,
            pltpu.roll(scaled, HEAD - HEAD // 4, 1),
            pltpu.roll(scaled, HEAD // 4, 1),
        )
        return scaled * cosine[...] + other * sine[...]

    def query_weights_here():
        incoming = several(0, n - 1, 0)
        remote(incoming, incoming, twin_ss.at[0], twin_rs.at[0], mate).wait_recv()

    def make_queries(first, count):
        raw = jnp.dot(
            normed[...].reshape(rows, width),
            wq[:, core, :, first * HEAD : (first + count) * HEAD].reshape(width, count * HEAD),
            preferred_element_type=jnp.float32,
        )
        for h in range(count):
            queries[first + h] = (turned(raw[:, h * HEAD : (h + 1) * HEAD], qg[...]) * HEAD ** (-0.5)).astype(
                jnp.bfloat16
            )

    def attend(a, b):
        for h in range(heads):
            q = queries[h]
            scores = [
                lax.dot_general(q, kv[i, 0], (((1,), (1,)), ((), ())), preferred_element_type=jnp.float32)
                for i in (a, b)
            ]
            old = peak[h]
            new = jnp.maximum(old, jnp.max(jnp.maximum(*scores), axis=1, keepdims=True))
            fade = jnp.exp(old - new)
            wide = jnp.concatenate([new] * (rows // HEAD), axis=1)
            parts = [jnp.exp(part - wide) for part in scores]
            peak[h] = new
            total[h] = fade * total[h] + jnp.sum(parts[0] + parts[1], axis=1, keepdims=True)
            summed[h] = (
                fade * summed[h]
                + jnp.dot(parts[0].astype(jnp.bfloat16), kv[a, 1], preferred_element_type=jnp.float32)
                + jnp.dot(parts[1].astype(jnp.bfloat16), kv[b, 1], preferred_element_type=jnp.float32)
            )

    @pl.when(core == 1)
    def _():
        for k in range(1, hops // FAR + 1):
            for way in (0, 1):
                if FAR * k <= reach[way]:
                    wkv_arrival(way, FAR * k).wait_recv()
                    wkv_send(way, FAR * k)
                    wkv_twin(way, FAR * k).start()
            for d in range(FAR * (k - 1) + 1, FAR * k):
                for way in (0, 1):
                    wkv_arrival(way, d).wait_recv()
                    wkv_twin(way, d).start()
        w_own_sends(1)
        for d in range(1, chips):
            normed_from(d).wait_recv()
        for d in range(chips):
            normed_from_mate(d).wait_recv()
        incoming = wkv.at[pl.ds(0, n - 1), pl.ds(0, wkv_half), :]
        remote(incoming, incoming, twin_ss.at[2], twin_rs.at[2], mate).wait_recv()
        projected = jnp.dot(
            normed[...].reshape(rows, width),
            wkv[...].reshape(width, 2 * HEAD),
            preferred_element_type=jnp.float32,
        )
        kv[z, 0] = turned(projected[:, :HEAD], kg[...]).astype(jnp.bfloat16)
        kv[z, 1] = projected[:, HEAD:].astype(jnp.bfloat16)
        for c in range(CHUNKS):
            kv_ring(0, z, 0, c).start()
            kv_ring(1, z, 0, c).start()
        for c in range(CHUNKS):
            kv_mate(0, z, 0, c).start()
        for d in range(1, chips):
            normed_mate(d).start()

        def kv_step(s):
            for c in range(CHUNKS):
                kv_ring(0, back(s), s - 1, c).wait_recv()
                kv_ring(0, back(s), s, c).start()
                kv_mate(0, back(s), s, c).start()
                kv_ring(1, ahead(s), s - 1, c).wait_recv()

                @pl.when(s < hops - 1)
                def _():
                    kv_ring(1, ahead(s), s, c).start()

                kv_mate(1, ahead(s), s, c).start()

        def early(s, carry):
            kv_step(s)
            return carry

        lax.fori_loop(1, LEAD + 1, early, 0)
        for h in range(heads):
            kv_step(LEAD + 1 + h)
            if h == 0:
                incoming = several(0, n - 1, 0)
                remote(incoming, incoming, md_ss.at[0], md_rs.at[0], mate).wait_recv()
                query_weights_here()
            make_queries(h, 1)
        lead = LEAD + heads
        pace = -(-(hops - 1) // (hops - 1 - lead))

        def pair(i, carry):
            attend(back(i), ahead(i))
            return carry

        def late(s, carry):
            kv_step(s)
            first = jnp.minimum(pace * (s - 1 - lead), s - 1) + 1
            lax.fori_loop(first, jnp.minimum(pace * (s - lead), s) + 1, pair, 0)
            return carry

        lax.fori_loop(lead + 1, hops, late, 0)
        for c in range(CHUNKS):
            kv_ring(0, back(hops), hops - 1, c).wait_recv()
            kv_mate(0, back(hops), hops, c).start()
        attend(z, back(hops))
        incoming = several(1, n - 1, 0)
        remote(incoming, incoming, md_ss.at[1], md_rs.at[1], mate).wait_recv()

    @pl.when(core == 0)
    def _():
        def w_step(f, k):
            w_arrival(f, 0, k - 1, MID).wait_recv()
            w_ring(f, 0, k, MID).start()
            w_ring(f, 0, k, 1).start()
            w_share(f, 0, MID * k)
            w_arrival(f, 1, k - 1, MID).wait_recv()

            @pl.when(MID * (k + 1) < hops)
            def _():
                w_ring(f, 1, k, MID).start()

            w_ring(f, 1, k, 1).start()
            w_share(f, 1, MID * k)
            for way in (0, 1):
                w_arrival(f, way, k - 1, 1).wait_recv()
                w_share(f, way, MID * k - 1)

        def w_end(f):
            k = hops // MID
            w_arrival(f, 0, k - 1, MID).wait_recv()
            w_share(f, 0, MID * k)
            for way in (0, 1):
                w_arrival(f, way, k - 1, 1).wait_recv()
                w_share(f, way, MID * k - 1)

        def query_step(k, carry):
            w_step(0, k)
            return carry

        def both_step(k, carry):
            w_step(0, k)
            w_step(1, k - middle + 1)
            return carry

        last = hops // MID
        middle = last // 2
        lax.fori_loop(1, middle - 1, query_step, 0)
        for d in range(1, chips):
            normed_from(d).wait_recv()
            normed_mate(d).start()
        w_step(0, middle - 1)
        w_own_sends(1)
        lax.fori_loop(middle, last, both_step, 0)
        w_end(0)
        for d in range(chips):
            normed_from_mate(d).wait_recv()
        query_weights_here()
        make_queries(0, heads)

        def pair(s, carry):
            kv_from_mate(0, back(s), s).wait_recv()
            kv_from_mate(1, ahead(s), s).wait_recv()
            attend(back(s), ahead(s))
            return carry

        def out_step(k, carry):
            w_step(1, k)
            return lax.fori_loop(2 * (k - done) - 1, 2 * (k - done) + 1, pair, carry)

        done = last - middle
        lax.fori_loop(done + 1, last, out_step, 0)
        w_end(1)
        lax.fori_loop(2 * (last - 1 - done) + 1, hops, pair, 0)
        kv_from_mate(0, z, 0).wait_recv()
        kv_from_mate(0, back(hops), hops).wait_recv()
        attend(z, back(hops))

    attended = jnp.concatenate([(summed[h] / total[h]).astype(jnp.bfloat16) for h in range(heads)], axis=1)
    incoming = several(1, n - 1, 0)
    remote(incoming, incoming, twin_ss.at[1], twin_rs.at[1], mate).wait_recv()

    per_piece = n // QUARTERS

    def term_mate(p):
        return remote(terms.at[p, 1 - core], partner_terms.at[p], td_ss.at[p], td_rs.at[p], mate)

    def project(p, carry):
        for j in range(per_piece // 2):
            first = p * per_piece + 2 * j
            both = jnp.concatenate([wo[first, core], wo[first + 1, core]], axis=1)
            term = jnp.dot(attended, both, preferred_element_type=jnp.float32).astype(jnp.bfloat16)
            for owner in range(n_tp):
                terms[p, owner % 2, owner // 2, :, 2 * j * cols : (2 * j + 2) * cols] = term[
                    owner * own_rows : (owner + 1) * own_rows
                ]
        term_mate(p).start()
        return carry

    lax.fori_loop(0, QUARTERS, project, 0)

    near = own_rows // 2
    upper, lower = pl.ds(0, near), pl.ds(near, near)
    ways = ((1, upper, lower), (chips - 1, lower, upper))

    def pair_sum(p, there, part):
        return terms[p, core, there, part].astype(jnp.float32) + partner_terms[p, there, part].astype(jnp.float32)

    def x_send(src, dst, p, way, i):
        return remote(src, dst, x_ss.at[p, way, i], x_rs.at[p, way, i], across[ways[way][0] - 1])

    def far_part(p, way):
        return x_send(pair_sums.at[p, way, 0], relayed.at[p, way], p, way, 0)

    def near_part(p, way):
        return x_send(pair_sums.at[p, way, 1], arrived.at[p, way, ways[way][2]], p, way, 1)

    def passed_part(p, way):
        return x_send(pair_sums.at[p, way, 2], arrived.at[p, way, ways[way][1]], p, way, 2)

    def send_sums(p):
        term_mate(p).wait_recv()
        for way, (on, passed, kept) in enumerate(ways):
            pair_sums[p, way, 0] = pair_sum(p, lax.rem(x + 2, chips), passed).astype(jnp.bfloat16)
            far_part(p, way).start()
        for way, (on, passed, kept) in enumerate(ways):
            pair_sums[p, way, 1] = pair_sum(p, lax.rem(x + on, chips), kept).astype(jnp.bfloat16)
            near_part(p, way).start()

    def pass_on(p):
        for way, (on, passed, kept) in enumerate(ways):
            far_part(p, way).wait_recv()
            both = pair_sum(p, lax.rem(x + on, chips), passed) + relayed[p, way].astype(jnp.float32)
            pair_sums[p, way, 2] = both.astype(jnp.bfloat16)
            passed_part(p, way).start()

    send_sums(0)
    for p in range(1, QUARTERS):
        send_sums(p)
        pass_on(p - 1)
    pass_on(QUARTERS - 1)
    piece_cols = per_piece * cols

    def out_copy(p):
        part = pl.ds(p * piece_cols, piece_cols)
        return pltpu.make_async_copy(mixed.at[:, part], out_hbm.at[:, part], out_sems.at[p])

    for p in range(QUARTERS):
        for way in (0, 1):
            near_part(p, way).wait_recv()
            passed_part(p, way).wait_recv()
        rows_sum = pair_sum(p, x, pl.ds(0, own_rows))
        for way in (0, 1):
            rows_sum = rows_sum + arrived[p, way].astype(jnp.float32)
        mixed[:, p * piece_cols : (p + 1) * piece_cols] = rows_sum.astype(mixed.dtype)
        out_copy(p).start()

    for p in range(QUARTERS):
        out_copy(p).wait()
    for d in range(1, chips):
        normed_to(d).wait_send()
    for d in range(chips):
        normed_mate(d).wait_send()

    @pl.when(core == 1)
    def _():
        for way in (0, 1):
            sends = sum(1 for d in range(0, reach[way], FAR) for j in range(1, FAR + 1) if d + j <= reach[way])
            sent = wkv.at[pl.ds(0, sends), pl.ds(0, wkv_half), :]
            remote(sent, sent, wkv_ss.at[way], wkv_rs.at[way, 0, 0], mate).wait_send()
            sent = kv.at[pl.ds(0, reach[way])]
            remote(sent, sent, kv_ss.at[way], kv_rs.at[way, 0, 0], mate).wait_send()
        sent = wkv.at[pl.ds(0, n - 1), pl.ds(0, wkv_half), :]
        remote(sent, sent, twin_ss.at[2], twin_rs.at[2], mate).wait_send()
        remote(kv, kv, kd_ss.at[0], kd_rs.at[0, 0], mate).wait_send()
        for f in (0, 1):
            sent = several(f, 2 * MID, 0)
            remote(sent, sent, w_ss.at[f], w_rs.at[f, 0, 0, 0], mate).wait_send()

    @pl.when(core == 0)
    def _():
        for f in (0, 1):
            sent = several(f, n - 1 - 2 * MID + MID)
            remote(sent, sent, w_ss.at[f], w_rs.at[f, 0, 0, 0], mate).wait_send()
            sent = several(f, n - 1)
            remote(sent, sent, twin_ss.at[f], twin_rs.at[f], mate).wait_send()
            sent = several(f, n - 1, 0)
            remote(sent, sent, md_ss.at[f], md_rs.at[f], mate).wait_send()

    for p in range(QUARTERS):
        term_mate(p).wait_send()
        for way in (0, 1):
            far_part(p, way).wait_send()
            near_part(p, way).wait_send()
            passed_part(p, way).wait_send()


def solution(mesh):
    n, n_tp = mesh.shape["sp"], mesh.shape["tp"]

    def local(tokens, input_gain, w_query, w_key, w_value, query_gain, key_gain, w_out):
        own_rows, width = tokens.shape
        rows = own_rows * n_tp
        depth, q_cols = w_query.shape
        heads = q_cols // HEAD
        out_rows, cols = w_out.shape
        chips = n_tp // 2
        hops = n // 2
        piece_cols = width // QUARTERS
        quarter = HEAD // 4
        inverse = 10000.0 ** (-np.arange(quarter) * 2.0 / (2 * quarter))
        inverse = jnp.asarray(np.tile(inverse, 4)[None, :].astype(np.float32))
        bf16, f32 = jnp.bfloat16, jnp.float32
        dma = pltpu.SemaphoreType.DMA
        return pl.pallas_call(
            functools.partial(fused, (n, n_tp)),
            out_shape=jax.ShapeDtypeStruct((own_rows, width), bf16),
            in_specs=[pl.BlockSpec(memory_space=pltpu.HBM)] * 9,
            out_specs=pl.BlockSpec(memory_space=pltpu.HBM),
            scratch_shapes=[
                pltpu.VMEM((own_rows, width), bf16),
                pltpu.VMEM((own_rows, width), bf16),
                pltpu.VMEM((1, width), f32),
                pltpu.VMEM((1, HEAD), f32),
                pltpu.VMEM((1, HEAD), f32),
                pltpu.VMEM((1, HEAD), f32),
                pltpu.VMEM((n_tp, own_rows, width), bf16),
                pltpu.VMEM((n, depth, 2 * HEAD), bf16),
                pltpu.VMEM((n, 2, depth, q_cols), bf16),
                pltpu.VMEM((n, 2, out_rows, cols), bf16),
                pltpu.VMEM((n, 2, rows, HEAD), bf16),
                pltpu.VMEM((rows, HEAD), f32),
                pltpu.VMEM((rows, HEAD), f32),
                pltpu.VMEM((heads, rows, HEAD), bf16),
                pltpu.VMEM((heads, rows, HEAD), f32),
                pltpu.VMEM((heads, rows, HEAD), f32),
                pltpu.VMEM((heads, rows, HEAD), f32),
                pltpu.VMEM((QUARTERS, 2, chips, own_rows, piece_cols), bf16),
                pltpu.VMEM((QUARTERS, chips, own_rows, piece_cols), bf16),
                pltpu.VMEM((QUARTERS, 2, 3, own_rows // 2, piece_cols), bf16),
                pltpu.VMEM((QUARTERS, 2, own_rows // 2, piece_cols), bf16),
                pltpu.VMEM((QUARTERS, 2, own_rows, piece_cols), bf16),
                dma((9,)),
                dma((QUARTERS,)),
                dma((chips - 1,)),
                dma((chips - 1,)),
                dma((chips,)),
                dma((chips,)),
                dma((2,)),
                dma((2, hops // FAR, FAR)),
                dma((2,)),
                dma((2, 2, hops // MID, MID)),
                dma((3,)),
                dma((3,)),
                dma((2,)),
                dma((2,)),
                dma((2,)),
                dma((2, hops, CHUNKS)),
                dma((1,)),
                dma((2, hops + 1)),
                dma((QUARTERS,)),
                dma((QUARTERS,)),
                dma((QUARTERS, 2, 3)),
                dma((QUARTERS, 2, 3)),
            ],
            compiler_params=pltpu.CompilerParams(
                collective_id=0, has_side_effects=True, vmem_limit_bytes=56 * 1024 * 1024
            ),
        )(
            tokens,
            input_gain[None, :],
            w_query,
            w_key,
            w_value,
            query_gain[None, :],
            key_gain[None, :],
            w_out,
            inverse,
        )

    in_specs = (
        P(("grp", "sp", "tp"), None),
        P(),
        P("sp", "tp"),
        P("sp", None),
        P("sp", None),
        P(),
        P(),
        P("tp", "sp"),
    )
    out_specs = P(("grp", "sp", "tp"), None)
    return jax.shard_map(local, mesh=mesh, in_specs=in_specs, out_specs=out_specs, check_vma=False)
```

time: 182 us -> 152 us (0.84)
  Pallas kernels: 175 us -> 149 us
  local copies, waits for them, and re-layouts: 6.52 us -> 1.67 us
    pallas_call x1, Pallas kernels: 175 us -> 149 us  [local(): pl.pallas_call(functools.partial(fused, (n, n_tp)), out_shape=jax.ShapeDt...]
    unnamed x17 -> x1, local copies, waits for them, and re-layouts: 6.43 us -> 1.67 us
where the time goes in v2:
time: 152 us; the launch traced here: 151 us
  Pallas kernels  149 us (98%)
  local copies, waits for them, and re-layouts  1.67 us (1%)
    pallas_call x1, Pallas kernels, local(): pl.pallas_call(functools.partial(fused, (n, n_tp)), out_shape=jax.ShapeDt...  149 us

profile of v2, /device:TPU:33, one launch (start us, length us, event | category | flops | bytes accessed | tf_op | source)
XLA Modules:
  0.0 151.2 jit_solution(967432555948684621)
XLA Ops:
  0.0 149.5 %shard_map.91 = bf16[32,4096]{1,0:T(8,128)(2,1)} custom-call(bf16[32,4096]{1,0:T(8,128)(2,1)} %tok_hbm.1, f32[1,4096]{1,0:T(1,128)} %bitcast.3, bf16[128,256]{1,0:T(8,128)(2,1)} %wq_hbm.1, bf16[128,512]{1,0:T(8,128)(2,1)} %wk_hbm.1, bf16[128,512]{1,0:T(8,128)(2,1)} %wv_hbm.1, f32[1,128]{1,0:T(1,128)} %bitcast.4, f32[1,128]{1,0:T(1,128)} %bitcast.5, ...), custom_call_target="tpu_custom_call" | custom-call | tf_op jit(solution)/shard_map/pallas_call | solution.py:605
  149.5 1.7 %copy.11 = bf16[32,4096]{1,0:T(8,128)(2,1)} copy(bf16[32,4096]{1,0:T(8,128)(2,1)} %shard_map.91) | data formatting | bytes 524288

commit v3 on v2

--- a/solution.py
+++ b/solution.py
@@ -61,6 +61,7 @@
     arrived,
     in_sems,
     out_sems,
+    left_sem,
     nx_ss,
     nx_rs,
     nd_ss,
@@ -132,13 +133,37 @@
     for load in loads:
         load.start()
 
-    peers = [mate, {"grp": other_grp}, {"grp": other_grp, "tp": other_t}] + across
-    peers += [{"sp": toward(way, j)} for way in (0, 1) for j in range(1, FAR + 1)]
-    peers += [{"sp": toward(way, j), "tp": other_t} for way in (0, 1) for j in range(1, MID + 1)]
     barrier = pltpu.get_barrier_semaphore()
-    for peer in peers:
-        pl.semaphore_signal(barrier, inc=1, device_id=peer, device_id_type=MESH)
-    pl.semaphore_wait(barrier, len(peers))
+
+    def say(semaphore, peers):
+        for peer in peers:
+            pl.semaphore_signal(semaphore, inc=1, device_id=peer, device_id_type=MESH)
+
+    level = [mate, {"grp": other_grp}, {"grp": other_grp, "tp": other_t}] + across
+    say(barrier, level)
+
+    def neighbours(way):
+        same = [{"sp": toward(way, j)} for j in range(1, FAR + 1)]
+        other = [{"sp": toward(way, j), "tp": other_t} for j in range(1, MID + 1)]
+        return same, other
+
+    def greet(way, semaphore, also):
+        same, other = neighbours(way)
+
+        @pl.when(core == 1)
+        def _():
+            say(semaphore, same + other[:also])
+
+        @pl.when(core == 0)
+        def _():
+            say(semaphore, same[:MID] + other)
+
+    greet(1, barrier, MID)
+    pl.semaphore_wait(barrier, len(level) + 2 * MID + core * (FAR - MID))
+    greet(0, left_sem, 0)
+
+    def left_is_in():
+        pl.semaphore_wait(left_sem, MID + core * FAR)
 
     wkv_half = wkv.shape[1] // 2
 
@@ -238,7 +263,6 @@
     @pl.when(core == 1)
     def _():
         wkv_send(0, 0)
-        wkv_send(1, 0)
 
     loads[2].wait()
     loads[3].wait()
@@ -249,14 +273,20 @@
         normed_to(d).start()
     normed_mate(0).start()
 
-    def w_own_sends(f):
-        loads[4 + f].wait()
+    def w_own_sends(f, way):
         for j in range(MID, 0, -1):
-            for way in (0, 1):
-                w_own(f, way, j).start()
-
-    w_own_sends(0)
-    for load in loads[6:]:
+            w_own(f, way, j).start()
+
+    loads[4].wait()
+    w_own_sends(0, 0)
+    left_is_in()
+
+    @pl.when(core == 1)
+    def _():
+        wkv_send(1, 0)
+
+    w_own_sends(0, 1)
+    for load in loads[5:]:
         load.wait()
 
     lane = lax.broadcasted_iota(jnp.int32, (rows, HEAD), 1)
@@ -298,21 +328,32 @@
             )
 
     def attend(a, b):
-        for h in range(heads):
-            q = queries[h]
-            scores = [
-                lax.dot_general(q, kv[i, 0], (((1,), (1,)), ((), ())), preferred_element_type=jnp.float32)
+        pieces = [(h, pl.ds(r, HEAD)) for h in range(heads) for r in range(0, rows, HEAD)]
+        scores = [
+            [
+                lax.dot_general(
+                    queries[h, part], kv[i, 0], (((1,), (1,)), ((), ())), preferred_element_type=jnp.float32
+                )
                 for i in (a, b)
             ]
-            old = peak[h]
-            new = jnp.maximum(old, jnp.max(jnp.maximum(*scores), axis=1, keepdims=True))
-            fade = jnp.exp(old - new)
+            for h, part in pieces
+        ]
+        peaks = []
+        for (h, part), pair in zip(pieces, scores):
+            highest = jnp.maximum(*pair)
+            highest = functools.reduce(
+                jnp.maximum, [highest[:, i : i + HEAD] for i in range(0, rows, HEAD)]
+            )
+            peaks.append(jnp.maximum(peak[h, part], jnp.max(highest, axis=1, keepdims=True)))
+        for (h, part), pair, new in zip(pieces, scores, peaks):
+            fade = jnp.exp(peak[h, part] - new)
             wide = jnp.concatenate([new] * (rows // HEAD), axis=1)
-            parts = [jnp.exp(part - wide) for part in scores]
-            peak[h] = new
-            total[h] = fade * total[h] + jnp.sum(parts[0] + parts[1], axis=1, keepdims=True)
-            summed[h] = (
-                fade * summed[h]
+            parts = [jnp.exp(score - wide) for score in pair]
+            peak[h, part] = new
+            added = parts[0] + parts[1]
+            total[h, part] = fade * total[h, part] + sum(added[:, i : i + HEAD] for i in range(0, rows, HEAD))
+            summed[h, part] = (
+                fade * summed[h, part]
                 + jnp.dot(parts[0].astype(jnp.bfloat16), kv[a, 1], preferred_element_type=jnp.float32)
                 + jnp.dot(parts[1].astype(jnp.bfloat16), kv[b, 1], preferred_element_type=jnp.float32)
             )
@@ -329,7 +370,8 @@
                 for way in (0, 1):
                     wkv_arrival(way, d).wait_recv()
                     wkv_twin(way, d).start()
-        w_own_sends(1)
+        w_own_sends(1, 0)
+        w_own_sends(1, 1)
         for d in range(1, chips):
             normed_from(d).wait_recv()
         for d in range(chips):
@@ -399,11 +441,11 @@
 
     @pl.when(core == 0)
     def _():
-        def w_step(f, k):
+        def w_step(f, k, share=w_share):
             w_arrival(f, 0, k - 1, MID).wait_recv()
             w_ring(f, 0, k, MID).start()
             w_ring(f, 0, k, 1).start()
-            w_share(f, 0, MID * k)
+            share(f, 0, MID * k)
             w_arrival(f, 1, k - 1, MID).wait_recv()
 
             @pl.when(MID * (k + 1) < hops)
@@ -411,10 +453,10 @@
                 w_ring(f, 1, k, MID).start()
 
             w_ring(f, 1, k, 1).start()
-            w_share(f, 1, MID * k)
+            share(f, 1, MID * k)
             for way in (0, 1):
                 w_arrival(f, way, k - 1, 1).wait_recv()
-                w_share(f, way, MID * k - 1)
+                share(f, way, MID * k - 1)
 
         def w_end(f):
             k = hops // MID
@@ -425,7 +467,7 @@
                 w_share(f, way, MID * k - 1)
 
         def query_step(k, carry):
-            w_step(0, k)
+            w_step(0, k, lambda f, way, d: None)
             return carry
 
         def both_step(k, carry):
@@ -439,8 +481,12 @@
         for d in range(1, chips):
             normed_from(d).wait_recv()
             normed_mate(d).start()
-        w_step(0, middle - 1)
-        w_own_sends(1)
+        query_step(middle - 1, 0)
+        w_own_sends(1, 0)
+        w_own_sends(1, 1)
+        for d in range(1, MID * middle - MID + 1):
+            for way in (0, 1):
+                w_share(0, way, d)
         lax.fori_loop(middle, last, both_step, 0)
         w_end(0)
         for d in range(chips):
@@ -466,7 +512,13 @@
         kv_from_mate(0, back(hops), hops).wait_recv()
         attend(z, back(hops))
 
-    attended = jnp.concatenate([(summed[h] / total[h]).astype(jnp.bfloat16) for h in range(heads)], axis=1)
+    attended = jnp.concatenate(
+        [
+            (summed[h] / jnp.sum(total[h], axis=1, keepdims=True)).astype(jnp.bfloat16)
+            for h in range(heads)
+        ],
+        axis=1,
+    )
     incoming = several(1, n - 1, 0)
     remote(incoming, incoming, twin_ss.at[1], twin_rs.at[1], mate).wait_recv()
 
@@ -632,6 +684,7 @@
                 pltpu.VMEM((QUARTERS, 2, own_rows, piece_cols), bf16),
                 dma((9,)),
                 dma((QUARTERS,)),
+                pltpu.SemaphoreType.REGULAR,
                 dma((chips - 1,)),
                 dma((chips - 1,)),
                 dma((chips,)),

time: 152 us -> 155 us (1.020)
  Pallas kernels: 149 us -> 153 us
    pallas_call x1, Pallas kernels: 149 us -> 153 us  [local(): pl.pallas_call(functools.partial(fused, (n, n_tp)), out_shape=jax.ShapeDt...]
where the time goes in v3:
time: 155 us
  Pallas kernels  153 us (99%)
  local copies, waits for them, and re-layouts  1.67 us (1%)
    pallas_call x1, Pallas kernels, local(): pl.pallas_call(functools.partial(fused, (n, n_tp)), out_shape=jax.ShapeDt...  153 us

profile of v3, /device:TPU:33, one launch (start us, length us, event | category | flops | bytes accessed | tf_op | source)
XLA Modules:
  0.0 154.7 jit_solution(11783888003290317123)
XLA Ops:
  0.0 153.0 %shard_map.91 = bf16[32,4096]{1,0:T(8,128)(2,1)} custom-call(bf16[32,4096]{1,0:T(8,128)(2,1)} %tok_hbm.1, f32[1,4096]{1,0:T(1,128)} %bitcast.3, bf16[128,256]{1,0:T(8,128)(2,1)} %wq_hbm.1, bf16[128,512]{1,0:T(8,128)(2,1)} %wk_hbm.1, bf16[128,512]{1,0:T(8,128)(2,1)} %wv_hbm.1, f32[1,128]{1,0:T(1,128)} %bitcast.4, f32[1,128]{1,0:T(1,128)} %bitcast.5, ...), custom_call_target="tpu_custom_call" | custom-call | tf_op jit(solution)/shard_map/pallas_call | solution.py:657
  153.0 1.7 %copy.11 = bf16[32,4096]{1,0:T(8,128)(2,1)} copy(bf16[32,4096]{1,0:T(8,128)(2,1)} %shard_map.91) | data formatting | bytes 524288

commit v4 on v2

--- a/solution.py
+++ b/solution.py
@@ -13,8 +13,9 @@
 EPS = 1e-06
 CHUNKS = 4
 FAR = 4
-MID = 2
-LEAD = 6
+MID = (2, 2)
+LEAD = 8
+ALONE = 4
 QUARTERS = 4
 MESH = pl.DeviceIdType.MESH
 
@@ -134,7 +135,7 @@
 
     peers = [mate, {"grp": other_grp}, {"grp": other_grp, "tp": other_t}] + across
     peers += [{"sp": toward(way, j)} for way in (0, 1) for j in range(1, FAR + 1)]
-    peers += [{"sp": toward(way, j), "tp": other_t} for way in (0, 1) for j in range(1, MID + 1)]
+    peers += [{"sp": toward(way, j), "tp": other_t} for way in (0, 1) for j in range(1, max(MID) + 1)]
     barrier = pltpu.get_barrier_semaphore()
     for peer in peers:
         pl.semaphore_signal(barrier, inc=1, device_id=peer, device_id_type=MESH)
@@ -180,11 +181,11 @@
         return remote(piece, piece, w_ss.at[f], w_rs.at[f, way, 0, j - 1], {"sp": toward(way, j), "tp": low_t})
 
     def w_ring(f, way, k, j):
-        piece = w_piece(f, source(way, MID * k))
+        piece = w_piece(f, source(way, MID[f] * k))
         return remote(piece, piece, w_ss.at[f], w_rs.at[f, way, k, j - 1], {"sp": toward(way, j)})
 
     def w_arrival(f, way, k, j):
-        piece = w_piece(f, source(way, MID * k + j))
+        piece = w_piece(f, source(way, MID[f] * k + j))
         return remote(piece, piece, w_ss.at[f], w_rs.at[f, way, k, j - 1], {"sp": toward(way, 1)})
 
     def w_share(f, way, d):
@@ -251,11 +252,10 @@
 
     def w_own_sends(f):
         loads[4 + f].wait()
-        for j in range(MID, 0, -1):
+        for j in range(MID[f], 0, -1):
             for way in (0, 1):
                 w_own(f, way, j).start()
 
-    w_own_sends(0)
     for load in loads[6:]:
         load.wait()
 
@@ -298,27 +298,39 @@
             )
 
     def attend(a, b):
-        for h in range(heads):
-            q = queries[h]
-            scores = [
-                lax.dot_general(q, kv[i, 0], (((1,), (1,)), ((), ())), preferred_element_type=jnp.float32)
+        pieces = [(h, pl.ds(r, HEAD)) for h in range(heads) for r in range(0, rows, HEAD)]
+        scores = [
+            [
+                lax.dot_general(
+                    queries[h, part], kv[i, 0], (((1,), (1,)), ((), ())), preferred_element_type=jnp.float32
+                )
                 for i in (a, b)
             ]
-            old = peak[h]
-            new = jnp.maximum(old, jnp.max(jnp.maximum(*scores), axis=1, keepdims=True))
-            fade = jnp.exp(old - new)
+            for h, part in pieces
+        ]
+        peaks = []
+        for (h, part), pair in zip(pieces, scores):
+            highest = jnp.maximum(*pair)
+            highest = functools.reduce(
+                jnp.maximum, [highest[:, i : i + HEAD] for i in range(0, rows, HEAD)]
+            )
+            peaks.append(jnp.maximum(peak[h, part], jnp.max(highest, axis=1, keepdims=True)))
+        for (h, part), pair, new in zip(pieces, scores, peaks):
+            fade = jnp.exp(peak[h, part] - new)
             wide = jnp.concatenate([new] * (rows // HEAD), axis=1)
-            parts = [jnp.exp(part - wide) for part in scores]
-            peak[h] = new
-            total[h] = fade * total[h] + jnp.sum(parts[0] + parts[1], axis=1, keepdims=True)
-            summed[h] = (
-                fade * summed[h]
+            parts = [jnp.exp(score - wide) for score in pair]
+            peak[h, part] = new
+            added = parts[0] + parts[1]
+            total[h, part] = fade * total[h, part] + sum(added[:, i : i + HEAD] for i in range(0, rows, HEAD))
+            summed[h, part] = (
+                fade * summed[h, part]
                 + jnp.dot(parts[0].astype(jnp.bfloat16), kv[a, 1], preferred_element_type=jnp.float32)
                 + jnp.dot(parts[1].astype(jnp.bfloat16), kv[b, 1], preferred_element_type=jnp.float32)
             )
 
     @pl.when(core == 1)
     def _():
+        w_own_sends(0)
         for k in range(1, hops // FAR + 1):
             for way in (0, 1):
                 if FAR * k <= reach[way]:
@@ -400,29 +412,33 @@
     @pl.when(core == 0)
     def _():
         def w_step(f, k):
-            w_arrival(f, 0, k - 1, MID).wait_recv()
-            w_ring(f, 0, k, MID).start()
-            w_ring(f, 0, k, 1).start()
-            w_share(f, 0, MID * k)
-            w_arrival(f, 1, k - 1, MID).wait_recv()
-
-            @pl.when(MID * (k + 1) < hops)
-            def _():
-                w_ring(f, 1, k, MID).start()
-
-            w_ring(f, 1, k, 1).start()
-            w_share(f, 1, MID * k)
-            for way in (0, 1):
-                w_arrival(f, way, k - 1, 1).wait_recv()
-                w_share(f, way, MID * k - 1)
+            mid = MID[f]
+            w_arrival(f, 0, k - 1, mid).wait_recv()
+            for j in range(mid, 0, -1):
+                w_ring(f, 0, k, j).start()
+            w_share(f, 0, mid * k)
+            w_arrival(f, 1, k - 1, mid).wait_recv()
+            if mid == 1:
+                pl.when(k + 1 < hops)(lambda: w_ring(f, 1, k, 1).start())
+            else:
+                pl.when(mid * (k + 1) < hops)(lambda: w_ring(f, 1, k, mid).start())
+                for j in range(mid - 1, 0, -1):
+                    w_ring(f, 1, k, j).start()
+            w_share(f, 1, mid * k)
+            for j in range(1, mid):
+                for way in (0, 1):
+                    w_arrival(f, way, k - 1, j).wait_recv()
+                    w_share(f, way, mid * (k - 1) + j)
 
         def w_end(f):
-            k = hops // MID
-            w_arrival(f, 0, k - 1, MID).wait_recv()
-            w_share(f, 0, MID * k)
-            for way in (0, 1):
-                w_arrival(f, way, k - 1, 1).wait_recv()
-                w_share(f, way, MID * k - 1)
+            mid = MID[f]
+            k = hops // mid
+            w_arrival(f, 0, k - 1, mid).wait_recv()
+            w_share(f, 0, mid * k)
+            for j in range(1, mid):
+                for way in (0, 1):
+                    w_arrival(f, way, k - 1, j).wait_recv()
+                    w_share(f, way, mid * (k - 1) + j)
 
         def query_step(k, carry):
             w_step(0, k)
@@ -430,18 +446,18 @@
 
         def both_step(k, carry):
             w_step(0, k)
-            w_step(1, k - middle + 1)
+            w_step(1, k - ALONE + 1)
             return carry
 
-        last = hops // MID
-        middle = last // 2
-        lax.fori_loop(1, middle - 1, query_step, 0)
+        q_last, o_last = hops // MID[0], hops // MID[1]
+        w_own_sends(0)
+        lax.fori_loop(1, min(3, ALONE), query_step, 0)
         for d in range(1, chips):
             normed_from(d).wait_recv()
             normed_mate(d).start()
-        w_step(0, middle - 1)
+        lax.fori_loop(min(3, ALONE), ALONE, query_step, 0)
         w_own_sends(1)
-        lax.fori_loop(middle, last, both_step, 0)
+        lax.fori_loop(ALONE, q_last, both_step, 0)
         w_end(0)
         for d in range(chips):
             normed_from_mate(d).wait_recv()
@@ -454,19 +470,29 @@
             attend(back(s), ahead(s))
             return carry
 
+        done = q_last - ALONE
+        each = -(-(hops - 1) // (o_last - 1 - done)) if o_last - 1 > done else hops
+
         def out_step(k, carry):
             w_step(1, k)
-            return lax.fori_loop(2 * (k - done) - 1, 2 * (k - done) + 1, pair, carry)
-
-        done = last - middle
-        lax.fori_loop(done + 1, last, out_step, 0)
+            i = k - done - 1
+            first = jnp.minimum(each * i, hops - 1) + 1
+            return lax.fori_loop(first, jnp.minimum(each * (i + 1), hops - 1) + 1, pair, carry)
+
+        lax.fori_loop(done + 1, o_last, out_step, 0)
         w_end(1)
-        lax.fori_loop(2 * (last - 1 - done) + 1, hops, pair, 0)
+        lax.fori_loop(min(each * max(o_last - 1 - done, 0), hops - 1) + 1, hops, pair, 0)
         kv_from_mate(0, z, 0).wait_recv()
         kv_from_mate(0, back(hops), hops).wait_recv()
         attend(z, back(hops))
 
-    attended = jnp.concatenate([(summed[h] / total[h]).astype(jnp.bfloat16) for h in range(heads)], axis=1)
+    attended = jnp.concatenate(
+        [
+            (summed[h] / jnp.sum(total[h], axis=1, keepdims=True)).astype(jnp.bfloat16)
+            for h in range(heads)
+        ],
+        axis=1,
+    )
     incoming = several(1, n - 1, 0)
     remote(incoming, incoming, twin_ss.at[1], twin_rs.at[1], mate).wait_recv()
 
@@ -564,13 +590,13 @@
         remote(sent, sent, twin_ss.at[2], twin_rs.at[2], mate).wait_send()
         remote(kv, kv, kd_ss.at[0], kd_rs.at[0, 0], mate).wait_send()
         for f in (0, 1):
-            sent = several(f, 2 * MID, 0)
+            sent = several(f, 2 * MID[f], 0)
             remote(sent, sent, w_ss.at[f], w_rs.at[f, 0, 0, 0], mate).wait_send()
 
     @pl.when(core == 0)
     def _():
         for f in (0, 1):
-            sent = several(f, n - 1 - 2 * MID + MID)
+            sent = several(f, n - 1 - MID[f])
             remote(sent, sent, w_ss.at[f], w_rs.at[f, 0, 0, 0], mate).wait_send()
             sent = several(f, n - 1)
             remote(sent, sent, twin_ss.at[f], twin_rs.at[f], mate).wait_send()
@@ -639,7 +665,7 @@
                 dma((2,)),
                 dma((2, hops // FAR, FAR)),
                 dma((2,)),
-                dma((2, 2, hops // MID, MID)),
+                dma((2, 2, hops // min(MID), max(MID))),
                 dma((3,)),
                 dma((3,)),
                 dma((2,)),

time: 152 us -> 152 us (level)
  no operation moved by 1% of the time
where the time goes in v4:
time: 152 us; the launch traced here: 151 us
  Pallas kernels  150 us (99%)
  local copies, waits for them, and re-layouts  1.67 us (1%)
    pallas_call x1, Pallas kernels, local(): pl.pallas_call(functools.partial(fused, (n, n_tp)), out_shape=jax.ShapeDt...  150 us

profile of v4, /device:TPU:33, one launch (start us, length us, event | category | flops | bytes accessed | tf_op | source)
XLA Modules:
  0.0 151.4 jit_solution(13539970484137563564)
XLA Ops:
  0.0 149.7 %shard_map.91 = bf16[32,4096]{1,0:T(8,128)(2,1)} custom-call(bf16[32,4096]{1,0:T(8,128)(2,1)} %tok_hbm.1, f32[1,4096]{1,0:T(1,128)} %bitcast.3, bf16[128,256]{1,0:T(8,128)(2,1)} %wq_hbm.1, bf16[128,512]{1,0:T(8,128)(2,1)} %wk_hbm.1, bf16[128,512]{1,0:T(8,128)(2,1)} %wv_hbm.1, f32[1,128]{1,0:T(1,128)} %bitcast.4, f32[1,128]{1,0:T(1,128)} %bitcast.5, ...), custom_call_target="tpu_custom_call" | custom-call | tf_op jit(solution)/shard_map/pallas_call | solution.py:631
  149.7 1.7 %copy.11 = bf16[32,4096]{1,0:T(8,128)(2,1)} copy(bf16[32,4096]{1,0:T(8,128)(2,1)} %shard_map.91) | data formatting | bytes 524288
